TPU v7x, 32 devices: a whole 2x2x4 slice. The times are simulated.
32 devices in a mesh: grp: 2 (over y), ep: 4 (over z), tp: 4 (over x, core).
Axes of the slice: x: 2, y: 2, z: 4, core: 2. Of those that a mesh axis runs over, the one named last changes fastest.
Arguments:
- queries: bfloat16 [2048, 2048], P(('grp', 'ep'), 'tp'), parts along dimension 0, may hold values from -8 to 8
- keys: bfloat16 [2048, 512], P(('grp', 'ep')), parts along dimension 0, may hold values from -8 to 8
- values: bfloat16 [2048, 512], P(('grp', 'ep')), parts along dimension 0, may hold values from -6 to 6
- q_gain: float32 [128], replicated, may hold values from 0.6 to 5.8
- k_gain: float32 [128], replicated, may hold values from 0.6 to 5.8
- w_out: bfloat16 [2048, 2048], P(None, 'tp'), may hold values from -0.125 to 0.125
- moe_rows: bfloat16 [1536, 2048], P(('grp', 'ep')), parts along dimension 0, may hold values from -6 to 6
- routes: int32 [1536, 2], P(('grp', 'ep')), parts along dimension 0, may hold values from 0 to 3, all different within a row; in each aligned block of 192 rows (0 to 191, 192 to 383, ...) at most 144 rows name the same one
- group_gate: float32 [1536], P(('grp', 'ep')), parts along dimension 0, may hold values from 0.25 to 1
- expert_logits: float32 [1536, 2], P(('grp', 'ep')), parts along dimension 0, may hold values from -6 to 6
- moe_gain: float32 [2048], replicated, may hold values from 0.1 to 1.9
- w_gate: bfloat16 [4, 2048, 2048], P('ep', None, 'tp'), may hold values from -0.125 to 0.125
- w_up: bfloat16 [4, 2048, 2048], P('ep', None, 'tp'), may hold values from -0.125 to 0.125
- w_down: bfloat16 [4, 2048, 2048], P('ep', 'tp'), may hold values from -0.125 to 0.125
Outputs:
- attn_out: bfloat16 [2048, 2048], P(('grp', 'ep'), 'tp'), parts along dimension 0
- moe_out: bfloat16 [1536, 2048], P(('grp', 'ep'), 'tp'), parts along dimension 0
There are 2 independent parts, one for each index of `grp`. A program takes and returns all parts, laid end to end along the dimension named above; an argument that names none is the same for every part. Nothing has to cross between parts.
Inputs may be any that keep to these rules, and one draw needn't show every extreme that they name: `routes`: each row names 2 different experts; within the rows of one index of ep no expert is named more than 144 times, a bound that some block reaches.
All inputs are finite; a program needn't handle non-finite values.
Results may differ from a plain program's by a relative error of at most 0.019.
The roundings to bfloat16 on the way count: a program that leaves them out, or rounds other values in their place, can miss the bound.
Values may be sent and summed in bfloat16 or wider, within the bound.
A program may use at most 64 MiB of HBM per device.

v0:
```python
import jax
import jax.numpy as jnp
from jax import lax
from jax.sharding import PartitionSpec as P

HEADS = 16
KV_HEADS = 4
HEAD_DIM = 128
GRID_W = 64
TOPK = 2


def head_norm(x, gain):
    wide = x.astype(jnp.float32)
    return wide * lax.rsqrt(jnp.mean(wide * wide, axis=-1, keepdims=True) + 1e-06) * gain


def rotate(x, first):
    count = x.shape[0]
    pos = first + jnp.arange(count, dtype=jnp.int32)
    row = (pos // GRID_W).astype(jnp.float32)
    col = (pos % GRID_W).astype(jnp.float32)
    nfreq = HEAD_DIM // 4
    inverse = 10000.0 ** (-jnp.arange(nfreq, dtype=jnp.float32) / nfreq)
    angle = jnp.concatenate(
        [
            row[:, None] * inverse,
            row[:, None] * inverse,
            col[:, None] * inverse,
            col[:, None] * inverse,
        ],
        axis=1,
    )
    parts = x.reshape(x.shape[:-1] + (2, 2, nfreq))
    turned = jnp.stack([-parts[..., 1, :], parts[..., 0, :]], axis=-2).reshape(x.shape)
    return x * jnp.cos(angle)[:, None, :] + turned * jnp.sin(angle)[:, None, :]


def per_device(
    queries,
    keys,
    values,
    q_gain,
    k_gain,
    w_out,
    moe_rows,
    routes,
    group_gate,
    expert_logits,
    moe_gain,
    w_gate,
    w_up,
    w_down,
):
    rows = queries.shape[0]
    heads_dev = queries.shape[1] // HEAD_DIM
    group = HEADS // KV_HEADS
    kv_dev = max(1, heads_dev // group)
    per_kv = heads_dev // kv_dev
    first_kv = lax.axis_index("tp") * heads_dev // group
    first_row = lax.axis_index("ep") * rows
    k_mine = lax.dynamic_slice_in_dim(keys, first_kv * HEAD_DIM, kv_dev * HEAD_DIM, 1)
    v_mine = lax.dynamic_slice_in_dim(values, first_kv * HEAD_DIM, kv_dev * HEAD_DIM, 1)
    k_rot = rotate(head_norm(k_mine.reshape(rows, kv_dev, HEAD_DIM), k_gain), first_row)
    k_rot = k_rot.astype(jnp.bfloat16).reshape(rows, kv_dev * HEAD_DIM)
    q_rot = rotate(head_norm(queries.reshape(rows, heads_dev, HEAD_DIM), q_gain), first_row)
    q_rot = q_rot.astype(jnp.bfloat16).reshape(rows, kv_dev, per_kv, HEAD_DIM)
    scale = HEAD_DIM ** (-0.5)
    top = jnp.full((rows, kv_dev, per_kv), -jnp.inf, jnp.float32)
    total = jnp.zeros((rows, kv_dev, per_kv), jnp.float32)
    acc = jnp.zeros((rows, kv_dev, per_kv, HEAD_DIM), jnp.float32)
    k_piece = lax.all_gather(k_rot, "ep", axis=0, tiled=True)
    v_piece = lax.all_gather(v_mine, "ep", axis=0, tiled=True)
    count = k_piece.shape[0]
    key_rows = k_piece.reshape(count, kv_dev, HEAD_DIM)
    value_rows = v_piece.reshape(count, kv_dev, HEAD_DIM)
    scores = (
        jnp.einsum("qkgd,nkd->qkgn", q_rot, key_rows, preferred_element_type=jnp.float32) * scale
    )
    new_top = jnp.max(scores, axis=-1)
    shrink = jnp.exp(top - new_top)
    expo = jnp.exp(scores - new_top[..., None])
    total = total * shrink + jnp.sum(expo, axis=-1)
    acc = acc * shrink[..., None] + jnp.einsum(
        "qkgn,nkd->qkgd", expo.astype(jnp.bfloat16), value_rows, preferred_element_type=jnp.float32
    )
    top, total, acc = (new_top, total, acc)
    mixed = (acc / total[..., None]).astype(jnp.bfloat16).reshape(rows, heads_dev * HEAD_DIM)
    attn_out = jnp.dot(
        lax.all_gather(mixed, "tp", axis=1, tiled=True), w_out, preferred_element_type=jnp.float32
    ).astype(jnp.bfloat16)
    count = moe_rows.shape[0]
    width = moe_rows.shape[1]
    peers = lax.axis_size("ep")
    capacity = 3 * count // peers
    wide = moe_rows.astype(jnp.float32)
    normed = (
        wide * lax.rsqrt(jnp.mean(wide * wide, axis=-1, keepdims=True) + 1e-06) * moe_gain
    ).astype(jnp.bfloat16)
    chosen = routes.reshape(-1)
    onehot = (chosen[:, None] == jnp.arange(peers, dtype=jnp.int32)[None, :]).astype(jnp.int32)
    rank = jnp.sum((jnp.cumsum(onehot, axis=0) - onehot) * onehot, axis=1)
    slots = chosen * capacity + rank
    owner = jnp.arange(count * TOPK, dtype=jnp.int32) // TOPK
    source = jnp.zeros((peers * capacity,), jnp.int32).at[slots].set(owner)
    used = jnp.zeros((peers * capacity,), jnp.bool_).at[slots].set(True)
    outgoing = jnp.where(used[:, None], normed[source], jnp.zeros((), jnp.bfloat16)).reshape(
        peers, capacity, width
    )
    part_cols = width // lax.axis_size("tp")
    mine = lax.dynamic_slice_in_dim(outgoing, lax.axis_index("tp") * part_cols, part_cols, 2)
    arrived = lax.all_gather(
        lax.all_to_all(mine, "ep", split_axis=0, concat_axis=0, tiled=True),
        "tp",
        axis=2,
        tiled=True,
    )
    first_dim, second_dim, cols = arrived.shape
    flat = arrived.reshape(first_dim * second_dim, cols)
    gate = jnp.dot(flat, w_gate[0], preferred_element_type=jnp.float32)
    up = jnp.dot(flat, w_up[0], preferred_element_type=jnp.float32)
    hidden = (jax.nn.silu(gate) * up).astype(jnp.bfloat16)
    result = jnp.dot(hidden, w_down[0], preferred_element_type=jnp.float32).astype(jnp.bfloat16)
    partial_value = result.reshape(first_dim, second_dim, cols)
    summed = (
        lax.psum_scatter(partial_value, "tp", scatter_dimension=2, tiled=True)
        .astype(jnp.float32)
        .astype(jnp.bfloat16)
    )
    back = lax.all_to_all(summed, "ep", split_axis=0, concat_axis=0, tiled=True)
    back = back.reshape(peers * capacity, back.shape[2])
    picked = back[slots].astype(jnp.float32).reshape(count, TOPK, back.shape[1])
    weights = group_gate[:, None] * jax.nn.softmax(expert_logits, axis=-1)
    moe_out = jnp.sum(weights[:, :, None] * picked, axis=1).astype(jnp.bfloat16)
    return (attn_out, moe_out)


def solution(mesh):
    placed = (
        P(("grp", "ep"), "tp"),
        P(("grp", "ep"), None),
        P(("grp", "ep"), None),
        P(),
        P(),
        P(None, "tp"),
        P(("grp", "ep"), None),
        P(("grp", "ep"), None),
        P(("grp", "ep")),
        P(("grp", "ep"), None),
        P(),
        P("ep", None, "tp"),
        P("ep", None, "tp"),
        P("ep", "tp", None),
    )
    return jax.shard_map(
        per_device,
        mesh=mesh,
        in_specs=placed,
        out_specs=(P(("grp", "ep"), "tp"), P(("grp", "ep"), "tp")),
        check_vma=False,
    )
```

profile of v0, /device:TPU:0, one launch (start us, length us, event | category | flops | bytes accessed | tf_op | source)
XLA Modules:
  0.0 148.1 jit_solution(11262557061539180350)
XLA Ops:
  7.2 0.9 copy.30
  9.2 1.2 reduce-window.6
  11.2 2.9 %scatter_custom_fusion.1 = s32[576]{0:T(1024)S(1)} fusion(s32[384]{0:T(512)S(1)} %fusion.58, s32[384]{0:T(512)S(1)} %add_select_fusion, s32[]{:T(128)} %constant.95.clone.1), kind=kCustom, calls=%fused_computation.81 | custom fusion | bytes 2308 | tf_op jit(solution)/shard_map/scatter | solution.py:105
  14.1 1.4 fusion.13
  15.5 2.0 %scatter_custom_fusion = pred[576]{0:T(1024)(128)(4,1)S(1)} fusion(s32[384]{0:T(512)S(1)} %fusion.58, pred[384]{0:T(512)(128)(4,1)S(1)} %broadcast.278, pred[]{:T(512)} %constant.115.clone.1), kind=kCustom, calls=%fused_computation.86 | custom fusion | bytes 577 | tf_op jit(solution)/shard_map/scatter | solution.py:106
  17.6 1.4 fusion.15
  19.0 4.0 %gather_fusion = bf16[576,2048]{1,0:T(8,128)(2,1)} fusion(bf16[192,2048]{1,0:T(8,128)(2,1)S(1)} %fusion.15, s32[1024]{0:T(1024)S(1)} %pad_clamp_fusion.1), kind=kCustom, calls=%fused_computation | custom fusion | bytes 4720896 | tf_op jit(solution)/shard_map/gather | solution.py:107
  23.0 1.3 dynamic-slice_select_fusion
  24.3 22.1 %all_to_all.10 = bf16[4,144,512]{2,1,0:T(8,128)(2,1)} all-to-all(bf16[4,144,512]{2,1,0:T(8,128)(2,1)S(1)} %dynamic-slice_select_fusion), channel_id=1, replica_groups=mesh['grp'=2,'ep'=4,'tp'=4] {'ep'}, dimensions={0} | all-to-all | bytes 1179648 | tf_op jit(solution)/shard_map/all_to_all | solution.py:113
  46.5 23.3 %all-gather.5.cloned.1.call-done = bf16[4,144,2048]{2,1,0:T(8,128)(2,1)} async-done(((bf16[4,144,512]{2,1,0:T(8,128)(2,1)}), bf16[4,144,2048]{2,1,0:T(8,128)(2,1)}) %all-gather.5.cloned.1.call-update) | async-done | bytes 2359312 | tf_op jit(solution)/shard_map/all_gather | solution.py:112
  69.7 4.7 %fusion.9 = f32[576,512]{1,0:T(8,128)} fusion(bf16[576,2048]{1,0:T(8,128)(2,1)} %bitcast.131, bf16[1,2048,512]{2,1,0:T(8,128)(2,1)} %param.25), kind=kOutput, calls=%fused_computation.15 | convolution fusion | flops 1207959552 | bytes 5636096 | tf_op jit(solution)/shard_map/dot_general | solution.py:120
  74.5 6.7 %convolution_convert_fusion = bf16[576,2048]{1,0:T(8,128)(2,1)} fusion(bf16[1,512,2048]{2,1,0:T(8,128)(2,1)S(1)} %copy-done, bf16[576,2048]{1,0:T(8,128)(2,1)} %bitcast.132, bf16[1,2048,512]{2,1,0:T(8,128)(2,1)} %param.26, f32[576,512]{1,0:T(8,128)} %fusion.9), kind=kOutput, calls=%fused_computation.9 | convolution fusion | flops 2418868224 | bytes 10092544 | tf_op jit(solution)/shard_map/dot_general | solution.py:123
  81.3 0.8 copy-done.2
  83.8 0.8 constant_dynamic-slice_fusion
  85.3 13.9 %all_gather.12 = bf16[1024,128]{1,0:T(8,128)(2,1)S(1)} all-gather(bf16[256,128]{1,0:T(8,128)(2,1)S(1)} %get-tuple-element.2), channel_id=1, replica_groups=mesh['grp'=2,'ep'=4,'tp'=4] {'ep'}, dimensions={0}, use_global_device_ids=true | all-gather | bytes 327680 | tf_op jit(solution)/shard_map/all_gather | solution.py:72
  99.2 14.7 %all_gather.13 = bf16[1024,128]{0,1:T(8,128)(2,1)S(1)} all-gather(bf16[256,128]{0,1:T(8,128)(2,1)S(1)} %copy.34), channel_id=1, replica_groups=mesh['grp'=2,'ep'=4,'tp'=4] {'ep'}, dimensions={0}, use_global_device_ids=true | all-gather | bytes 327680 | tf_op jit(solution)/shard_map/all_gather | solution.py:73
  113.9 0.7 bitcast_reduce_fusion
  114.6 0.7 fusion.1
  115.4 1.6 %fusion.31 = bf16[1,128,256,4]{2,1,3,0:T(8,128)(2,1)} fusion(f32[1024,256,4]{1,0,2:T(8,128)S(1)} %get-tuple-element.14, f32[256,4]{0,1:T(4,128)S(1)} %get-tuple-element.13, bf16[1024,128]{0,1:T(8,128)(2,1)S(1)} %all_gather.13, f32[256,4]{0,1:T(4,128)S(1)} %get-tuple-element.10, f32[256,4]{0,1:T(4,128)S(1)} %get-tuple-element.9), kind=kOutput, calls=%fused_computation.30 | convolution fusion | flops 271974400 | bytes 4730880 | tf_op jit(solution)/shard_map/qkgn,nkd->qkgd/dot_general | solution.py:84
  117.0 4.8 %all-to-all-start.1 = ((bf16[4,144,512]{2,1,0:T(8,128)(2,1)}), bf16[4,144,512]{2,1,0:T(8,128)(2,1)S(1)}, u32[]{:S(2)}, u32[]{:S(2)}) async-start(bf16[4,144,512]{2,1,0:T(8,128)(2,1)} %reduce-scatter.2.cloned.1.call-done), calls=%async_computation.2 | async-start | bytes 1179648 | tf_op jit(solution)/shard_map/all_to_all | solution.py:130
  122.0 12.0 %all-gather.3.cloned.1.call-done = bf16[256,2048]{0,1:T(8,128)(2,1)} async-done(((bf16[256,512]{0,1:T(8,128)(2,1)}), bf16[256,2048]{0,1:T(8,128)(2,1)}) %all-gather.3.cloned.1.call-update) | async-done | bytes 1048592 | tf_op jit(solution)/shard_map/all_gather | solution.py:90
  134.0 3.3 %convolution_convert_fusion.1 = bf16[256,512]{1,0:T(8,128)(2,1)} fusion(bf16[256,2048]{0,1:T(8,128)(2,1)} %all-gather.3.cloned.1.call-done, bf16[2048,512]{1,0:T(8,128)(2,1)} %param.19), kind=kOutput, calls=%fused_computation.28 | convolution fusion | flops 537001984 | bytes 3407872 | tf_op jit(solution)/shard_map/dot_general | solution.py:89
  137.3 2.1 %gather_fusion.1 = bf16[384,512]{1,0:T(8,128)(2,1)S(1)} fusion(bf16[576,512]{1,0:T(8,128)(2,1)S(1)} %bitcast.122, s32[1024]{0:T(1024)S(1)} %pad_clamp_fusion), kind=kCustom, calls=%fused_computation.1 | custom fusion | bytes 787968 | tf_op jit(solution)/shard_map/gather | solution.py:132
  139.9 1.7 %multiply_reduce_fusion = bf16[192,512]{1,0:T(8,128)(2,1)} fusion(f32[192,2,512]{2,1,0:T(2,128)S(1)} %reshape.352, f32[192,2]{1,0:T(8,128)S(1)} %copy.28), kind=kLoop, calls=%fused_computation.31 | loop fusion | flops 294912 | bytes 984576 | tf_op jit(solution)/shard_map/reduce_sum | solution.py:134
  (68 shorter events, 4.9 us)
Async XLA Ops:
  7.2 67.3 %copy-start = (bf16[1,512,2048]{2,1,0:T(8,128)(2,1)S(1)}, bf16[1,512,2048]{2,1,0:T(8,128)(2,1)}, u32[]{:S(2)}) copy-start(bf16[1,512,2048]{2,1,0:T(8,128)(2,1)} %param.27) | copy-start | bytes 6291460
  7.2 62.6 %all-gather.5.cloned.1.call-start = ((), (), s32[]{:S(2)}) async-start(), calls=%async_computation.4 | async-start | bytes 2949120 | tf_op jit(solution)/shard_map/all_gather | solution.py:112
  46.4 70.6 %reduce-scatter.2.cloned.1.call-start = ((), (), s32[]{:S(2)}) async-start(), calls=%async_computation.5 | async-start | bytes 2949120 | tf_op jit(solution)/shard_map/reduce_scatter | solution.py:126
  81.2 0.9 copy-start.2
  81.2 1.1 copy-start.4
  81.2 2.4 %copy-start.1 = (bf16[256,512]{1,0:T(8,128)(2,1)S(1)}, bf16[256,512]{1,0:T(8,128)(2,1)}, u32[]{:S(2)}) copy-start(bf16[256,512]{1,0:T(8,128)(2,1)} %param.14) | copy-start | bytes 786436
  81.2 2.5 %copy-start.5 = (f32[128]{0:T(128)S(1)}, f32[128]{0:T(128)}, u32[]{:S(2)}) copy-start(f32[128]{0:T(128)} %param.17) | copy-start | bytes 1540
  81.2 52.8 %all-gather.3.cloned.1.call-start = ((), (), s32[]{:S(2)}) async-start(), calls=%async_computation.3 | async-start | bytes 1310720 | tf_op jit(solution)/shard_map/all_gather | solution.py:90
  115.3 6.4 %copy-start.3 = (f32[192,2]{0,1:T(2,128)S(1)}, f32[192,2]{0,1:T(2,128)}, u32[]{:S(2)}) copy-start(f32[192,2]{0,1:T(2,128)} %param.23) | copy-start | bytes 4612
  115.3 6.5 %copy-start.6 = (f32[192]{0:T(256)S(1)}, f32[192]{0:T(256)}, u32[]{:S(2)}) copy-start(f32[192]{0:T(256)} %param.22) | copy-start | bytes 2308
  117.0 20.3 %all-to-all-start.1 = ((bf16[4,144,512]{2,1,0:T(8,128)(2,1)}), bf16[4,144,512]{2,1,0:T(8,128)(2,1)S(1)}, u32[]{:S(2)}, u32[]{:S(2)}) async-start(bf16[4,144,512]{2,1,0:T(8,128)(2,1)} %reduce-scatter.2.cloned.1.call-done), calls=%async_computation.2 | async-start | bytes 1179648 | tf_op jit(solution)/shard_map/all_to_all | solution.py:130
Sparse Core Ops, SparseCore 0:
  46.5 23.1 all-gather.4
  81.3 32.7 reduce-scatter.1
  117.1 16.8 all-gather.2
where the time goes:
time: 149 us; the launch traced here: 148 us
  blocking collectives  50.8 us (34%)
  waiting for transfers between devices  35.3 us (24%)
  matrix products  17.1 us (11%)
  local copies, waits for them, and re-layouts  15.8 us (11%)
  between operations  14.1 us (9%)
  other arithmetic  10.1 us (7%)
  starting transfers between devices  4.88 us (3%)
    all_gather x1, waiting for transfers between devices, per_device(): lax.all_gather(lax.all_to_all(mine, 'ep', split_axis=0, concat_axis=0, ti...  23.3 us
    all_to_all x1, blocking collectives, per_device(): lax.all_to_all(mine, 'ep', split_axis=0, concat_axis=0, tiled=True)  22.1 us
    all_gather x1, blocking collectives, per_device(): v_piece = lax.all_gather(v_mine, 'ep', axis=0, tiled=True)  14.7 us
    all_gather x1, blocking collectives, per_device(): k_piece = lax.all_gather(k_rot, 'ep', axis=0, tiled=True)  13.9 us
    all_gather x1, waiting for transfers between devices, per_device(): lax.all_gather(mixed, 'tp', axis=1, tiled=True)  12 us
    dot_general x1, matrix products, per_device(): jnp.dot(hidden, w_down[0], preferred_element_type=jnp.float32)  6.71 us
    all_to_all x1, starting transfers between devices, per_device(): back = lax.all_to_all(summed, 'ep', split_axis=0, concat_axis=0, tiled=True)  4.76 us
    dot_general x1, matrix products, per_device(): gate = jnp.dot(flat, w_gate[0], preferred_element_type=jnp.float32)  4.74 us
  transfers between devices with their start and end apart: 4, of which 2 were waited for; matrix products, arithmetic and copies ran while one was open for 6% of the time, Pallas kernels for 0%

commit v1 on v0

--- a/solution.py
+++ b/solution.py
@@ -87,7 +87,9 @@
     top, total, acc = (new_top, total, acc)
     mixed = (acc / total[..., None]).astype(jnp.bfloat16).reshape(rows, heads_dev * HEAD_DIM)
     attn_out = jnp.dot(
-        lax.all_gather(mixed, "tp", axis=1, tiled=True), w_out, preferred_element_type=jnp.float32
+        jnp.concatenate(lax.all_gather(mixed, "tp"), axis=1),
+        w_out,
+        preferred_element_type=jnp.float32,
     ).astype(jnp.bfloat16)
     count = moe_rows.shape[0]
     width = moe_rows.shape[1]

time: 149 us -> 151 us (1.013)
  local copies, waits for them, and re-layouts: 15.8 us -> 18.9 us
    all_gather x0 -> x1, local copies, waits for them, and re-layouts: none -> 2.27 us  [per_device(): lax.all_gather(mixed, 'tp')]
  transfers between devices with their start and end apart: 4 -> 4, of which waited for: 2 -> 2; matrix products, arithmetic and copies ran while one was open for 6% -> 8% of each run, Pallas kernels for 0% -> 0%
where the time goes in v1:
time: 151 us
  blocking collectives  50.8 us (34%)
  waiting for transfers between devices  35.3 us (23%)
  local copies, waits for them, and re-layouts  18.9 us (13%)
  matrix products  16.4 us (11%)
  between operations  14.1 us (9%)
  other arithmetic  10.1 us (7%)
  starting transfers between devices  4.88 us (3%)
    all_gather x1, waiting for transfers between devices, per_device(): lax.all_gather(lax.all_to_all(mine, 'ep', split_axis=0, concat_axis=0, ti...  23.3 us
    all_to_all x1, blocking collectives, per_device(): lax.all_to_all(mine, 'ep', split_axis=0, concat_axis=0, tiled=True)  22.1 us
    all_gather x1, blocking collectives, per_device(): v_piece = lax.all_gather(v_mine, 'ep', axis=0, tiled=True)  14.7 us
    all_gather x1, blocking collectives, per_device(): k_piece = lax.all_gather(k_rot, 'ep', axis=0, tiled=True)  13.9 us
    all_gather x1, waiting for transfers between devices, per_device(): lax.all_gather(mixed, 'tp')  12 us
    dot_general x1, matrix products, per_device(): jnp.dot(hidden, w_down[0], preferred_element_type=jnp.float32)  6.71 us
    all_to_all x1, starting transfers between devices, per_device(): back = lax.all_to_all(summed, 'ep', split_axis=0, concat_axis=0, tiled=True)  4.76 us
    dot_general x1, matrix products, per_device(): gate = jnp.dot(flat, w_gate[0], preferred_element_type=jnp.float32)  4.74 us
  transfers between devices with their start and end apart: 4, of which 2 were waited for; matrix products, arithmetic and copies ran while one was open for 8% of the time, Pallas kernels for 0%

profile of v1, /device:TPU:0, one launch (start us, length us, event | category | flops | bytes accessed | tf_op | source)
XLA Modules:
  0.0 150.6 jit_solution(17899786953340325063)
XLA Ops:
  7.2 0.9 copy.57
  9.2 1.2 reduce-window.6
  11.2 2.9 %scatter_custom_fusion.1 = s32[576]{0:T(1024)S(1)} fusion(s32[384]{0:T(512)S(1)} %fusion.58, s32[384]{0:T(512)S(1)} %add_select_fusion, s32[]{:T(128)} %constant.95.clone.1), kind=kCustom, calls=%fused_computation.81 | custom fusion | bytes 2308 | tf_op jit(solution)/shard_map/scatter | solution.py:107
  14.1 1.4 fusion.13
  15.5 2.0 %scatter_custom_fusion = pred[576]{0:T(1024)(128)(4,1)S(1)} fusion(s32[384]{0:T(512)S(1)} %fusion.58, pred[384]{0:T(512)(128)(4,1)S(1)} %broadcast.278, pred[]{:T(512)} %constant.115.clone.1), kind=kCustom, calls=%fused_computation.86 | custom fusion | bytes 577 | tf_op jit(solution)/shard_map/scatter | solution.py:108
  17.6 1.4 fusion.15
  19.0 4.0 %gather_fusion = bf16[576,2048]{1,0:T(8,128)(2,1)} fusion(bf16[192,2048]{1,0:T(8,128)(2,1)S(1)} %fusion.15, s32[1024]{0:T(1024)S(1)} %pad_clamp_fusion.1), kind=kCustom, calls=%fused_computation | custom fusion | bytes 4720896 | tf_op jit(solution)/shard_map/gather | solution.py:109
  23.0 1.3 dynamic-slice_select_fusion
  24.3 22.1 %all_to_all.10 = bf16[4,144,512]{2,1,0:T(8,128)(2,1)} all-to-all(bf16[4,144,512]{2,1,0:T(8,128)(2,1)S(1)} %dynamic-slice_select_fusion), channel_id=1, replica_groups=mesh['grp'=2,'ep'=4,'tp'=4] {'ep'}, dimensions={0} | all-to-all | bytes 1179648 | tf_op jit(solution)/shard_map/all_to_all | solution.py:115
  46.5 23.3 %all-gather.5.cloned.1.call-done = bf16[4,144,2048]{2,1,0:T(8,128)(2,1)} async-done(((bf16[4,144,512]{2,1,0:T(8,128)(2,1)}), bf16[4,144,2048]{2,1,0:T(8,128)(2,1)}) %all-gather.5.cloned.1.call-update) | async-done | bytes 2359312 | tf_op jit(solution)/shard_map/all_gather | solution.py:114
  69.7 4.7 %fusion.9 = f32[576,512]{1,0:T(8,128)} fusion(bf16[576,2048]{1,0:T(8,128)(2,1)} %bitcast.135, bf16[1,2048,512]{2,1,0:T(8,128)(2,1)} %param.25), kind=kOutput, calls=%fused_computation.15 | convolution fusion | flops 1207959552 | bytes 5636096 | tf_op jit(solution)/shard_map/dot_general | solution.py:122
  74.5 6.7 %convolution_convert_fusion = bf16[576,2048]{1,0:T(8,128)(2,1)} fusion(bf16[1,512,2048]{2,1,0:T(8,128)(2,1)S(1)} %copy-done, bf16[576,2048]{1,0:T(8,128)(2,1)} %bitcast.136, bf16[1,2048,512]{2,1,0:T(8,128)(2,1)} %param.26, f32[576,512]{1,0:T(8,128)} %fusion.9), kind=kOutput, calls=%fused_computation.9 | convolution fusion | flops 2418868224 | bytes 10092544 | tf_op jit(solution)/shard_map/dot_general | solution.py:125
  81.3 0.8 copy-done.2
  83.8 0.8 constant_dynamic-slice_fusion
  85.3 13.9 %all_gather.12 = bf16[1024,128]{1,0:T(8,128)(2,1)S(1)} all-gather(bf16[256,128]{1,0:T(8,128)(2,1)S(1)} %get-tuple-element.2), channel_id=1, replica_groups=mesh['grp'=2,'ep'=4,'tp'=4] {'ep'}, dimensions={0}, use_global_device_ids=true | all-gather | bytes 327680 | tf_op jit(solution)/shard_map/all_gather | solution.py:72
  99.2 14.7 %all_gather.13 = bf16[1024,128]{0,1:T(8,128)(2,1)S(1)} all-gather(bf16[256,128]{0,1:T(8,128)(2,1)S(1)} %copy.61), channel_id=1, replica_groups=mesh['grp'=2,'ep'=4,'tp'=4] {'ep'}, dimensions={0}, use_global_device_ids=true | all-gather | bytes 327680 | tf_op jit(solution)/shard_map/all_gather | solution.py:73
  115.4 0.9 fusion.31
  116.3 0.8 copy.53
  117.2 4.8 %all-to-all-start.1 = ((bf16[4,144,512]{2,1,0:T(8,128)(2,1)}), bf16[4,144,512]{2,1,0:T(8,128)(2,1)S(1)}, u32[]{:S(2)}, u32[]{:S(2)}) async-start(bf16[4,144,512]{2,1,0:T(8,128)(2,1)} %reduce-scatter.2.cloned.1.call-done), calls=%async_computation.2 | async-start | bytes 1179648 | tf_op jit(solution)/shard_map/all_to_all | solution.py:132
  122.1 12.0 %all-gather.3.cloned.1.call-done = bf16[4,256,512]{2,1,0:T(8,128)(2,1)} async-done(((bf16[1,256,512]{2,1,0:T(8,128)(2,1)}), bf16[4,256,512]{2,1,0:T(8,128)(2,1)}) %all-gather.3.cloned.1.call-update) | async-done | bytes 1048592 | tf_op jit(solution)/shard_map/all_gather | solution.py:90
  134.1 2.3 %copy.54 = bf16[4,256,512]{1,2,0:T(8,128)(2,1)} copy(bf16[4,256,512]{2,1,0:T(8,128)(2,1)} %all-gather.3.cloned.1.call-done) | data formatting | bytes 2097152 | tf_op jit(solution)/shard_map/all_gather | solution.py:90
  136.4 3.3 %convolution_convert_fusion.1 = bf16[256,512]{1,0:T(8,128)(2,1)} fusion(bf16[256,2048]{0,1:T(8,128)(2,1)} %bitcast.129, bf16[2048,512]{1,0:T(8,128)(2,1)} %param.19), kind=kOutput, calls=%fused_computation.28 | convolution fusion | flops 537001984 | bytes 3407872 | tf_op jit(solution)/shard_map/dot_general | solution.py:89
  139.8 2.1 %gather_fusion.1 = bf16[384,512]{1,0:T(8,128)(2,1)S(1)} fusion(bf16[576,512]{1,0:T(8,128)(2,1)S(1)} %bitcast.125, s32[1024]{0:T(1024)S(1)} %pad_clamp_fusion), kind=kCustom, calls=%fused_computation.1 | custom fusion | bytes 787968 | tf_op jit(solution)/shard_map/gather | solution.py:134
  142.3 1.7 %multiply_reduce_fusion = bf16[192,512]{1,0:T(8,128)(2,1)} fusion(f32[192,2,512]{2,1,0:T(2,128)S(1)} %reshape.356, f32[192,2]{1,0:T(8,128)S(1)} %copy.55), kind=kLoop, calls=%fused_computation.31 | loop fusion | flops 294912 | bytes 984576 | tf_op jit(solution)/shard_map/reduce_sum | solution.py:136
  (70 shorter events, 6.3 us)
Async XLA Ops:
  7.2 67.3 %copy-start = (bf16[1,512,2048]{2,1,0:T(8,128)(2,1)S(1)}, bf16[1,512,2048]{2,1,0:T(8,128)(2,1)}, u32[]{:S(2)}) copy-start(bf16[1,512,2048]{2,1,0:T(8,128)(2,1)} %param.27) | copy-start | bytes 6291460
  7.2 62.6 %all-gather.5.cloned.1.call-start = ((), (), s32[]{:S(2)}) async-start(), calls=%async_computation.4 | async-start | bytes 2949120 | tf_op jit(solution)/shard_map/all_gather | solution.py:114
  46.4 70.7 %reduce-scatter.2.cloned.1.call-start = ((), (), s32[]{:S(2)}) async-start(), calls=%async_computation.5 | async-start | bytes 2949120 | tf_op jit(solution)/shard_map/reduce_scatter | solution.py:128
  81.2 0.9 copy-start.2
  81.2 1.1 copy-start.4
  81.2 2.4 %copy-start.1 = (bf16[256,512]{1,0:T(8,128)(2,1)S(1)}, bf16[256,512]{1,0:T(8,128)(2,1)}, u32[]{:S(2)}) copy-start(bf16[256,512]{1,0:T(8,128)(2,1)} %param.14) | copy-start | bytes 786436
  81.2 2.5 %copy-start.5 = (f32[128]{0:T(128)S(1)}, f32[128]{0:T(128)}, u32[]{:S(2)}) copy-start(f32[128]{0:T(128)} %param.17) | copy-start | bytes 1540
  81.2 52.9 %all-gather.3.cloned.1.call-start = ((), (), s32[]{:S(2)}) async-start(), calls=%async_computation.3 | async-start | bytes 1310720 | tf_op jit(solution)/shard_map/all_gather | solution.py:90
  115.3 6.6 %copy-start.3 = (f32[192,2]{0,1:T(2,128)S(1)}, f32[192,2]{0,1:T(2,128)}, u32[]{:S(2)}) copy-start(f32[192,2]{0,1:T(2,128)} %param.23) | copy-start | bytes 4612
  115.3 6.6 %copy-start.6 = (f32[192]{0:T(256)S(1)}, f32[192]{0:T(256)}, u32[]{:S(2)}) copy-start(f32[192]{0:T(256)} %param.22) | copy-start | bytes 2308
  117.2 22.6 %all-to-all-start.1 = ((bf16[4,144,512]{2,1,0:T(8,128)(2,1)}), bf16[4,144,512]{2,1,0:T(8,128)(2,1)S(1)}, u32[]{:S(2)}, u32[]{:S(2)}) async-start(bf16[4,144,512]{2,1,0:T(8,128)(2,1)} %reduce-scatter.2.cloned.1.call-done), calls=%async_computation.2 | async-start | bytes 1179648 | tf_op jit(solution)/shard_map/all_to_all | solution.py:132
Sparse Core Ops, SparseCore 0:
  46.5 23.1 all-gather.4
  81.3 32.7 reduce-scatter.1
  117.2 16.8 all-gather.2
